TPU v7x, 32 devices: a whole 2x2x4 slice. The times are simulated.
32 devices in a mesh: ep: 8 (over z, x), tp: 4 (over y, core).
Axes of the slice: x: 2, y: 2, z: 4, core: 2. Of those that a mesh axis runs over, the one named last changes fastest.
Arguments:
- pool_in: bfloat16 [8192, 1024], P(('ep', 'tp')), may hold values from -6 to 6
- w_pool: bfloat16 [8, 128, 128], replicated, may hold values from -0.5 to 0.5
- pool_scale: float32 [1024], replicated, may hold values from 0.1 to 1.9
- w_out: bfloat16 [1024, 2048], replicated, may hold values from -0.1875 to 0.1875
- expert_in: bfloat16 [4096, 2048], P('ep'), may hold values from -6 to 6
- ffn_gain: float32 [2048], replicated, may hold values from 0.1 to 1.9
- routes: int32 [4096, 2], P('ep'), may hold values from 0 to 7, all different within a row; in each aligned block of 128 rows (0 to 127, 128 to 255, ...) at most 48 rows name the same one
- route_weight: float32 [4096, 2], P('ep'), may hold values from 0.25 to 1
- w_gate: bfloat16 [8, 2048, 1024], P('ep', None, 'tp'), may hold values from -0.125 to 0.125
- w_up: bfloat16 [8, 2048, 1024], P('ep', None, 'tp'), may hold values from -0.125 to 0.125
- w_down: bfloat16 [8, 1024, 2048], P('ep', 'tp'), may hold values from -0.1875 to 0.1875
Outputs:
- mixer_out: bfloat16 [8192, 2048], P(('ep', 'tp'))
- expert_out: bfloat16 [4096, 2048], P(('ep', 'tp'))
Inputs may be any that keep to these rules, and one draw needn't show every extreme that they name: `routes`: each row names 2 different experts. In each aligned block of 128 rows no expert is named by more than 48 rows, and in some block some expert is named by exactly 48 rows.
All inputs are finite; a program needn't handle non-finite values.
Results may differ from a plain program's by a relative error of at most 0.012.
Values may be sent and summed in bfloat16 or wider, within the bound.
A program may use at most 128 MiB of HBM per device.

v0:
```python
import functools

import jax
import jax.numpy as jnp
from jax import lax
from jax.experimental import pallas as pl
from jax.experimental.pallas import tpu as pltpu
from jax.sharding import PartitionSpec as P

GDIM = 128
WMAX = 16
K = 2
EPS = 0.05
MESH = pl.DeviceIdType.MESH
F32 = jnp.float32
BF16 = jnp.bfloat16
LANES = 128


def dot(a, b):
    return jnp.dot(a, b, preferred_element_type=F32)


def kernel(
    dims,
    routes_ref,
    weight_ref,
    gain_ref,
    scale_ref,
    wpool_hbm,
    pool_hbm,
    wout_hbm,
    rows_hbm,
    gate_hbm,
    up_hbm,
    down_hbm,
    mixer_v,
    expert_v,
    wpool_ref,
    pool_v,
    halo_v,
    wout_v,
    scaled_v,
    mine_v,
    normed_v,
    outgoing,
    arrived,
    gate_all,
    up_all,
    gate_sum,
    up_sum,
    hidden,
    down_all,
    result,
    returned,
    local_sem,
    far_s,
    far_r,
    near_s,
    near_r,
    relay_s,
    relay_r,
    go_s,
    go_r,
    back_s,
    back_r,
    halo_s,
    halo_r,
):
    ep_n, tp_n, cap, gate_n, down_n = dims
    me = lax.axis_index("ep")
    own = lax.axis_index("tp")
    near = own + 1 - 2 * (own % 2)
    far = (own + tp_n // 2) % tp_n
    index = me * tp_n + own
    total = ep_n * tp_n
    after = (index + 1) % total
    before = (index + total - 1) % total
    block_rows, width = mine_v.shape
    slots = ep_n * cap
    local = gate_hbm.shape[2]
    deep = width // gate_n
    part = width // down_n

    def partner(i):
        return (me + ep_n // 2 + ((i + 1) // 2) * (1 - 2 * (i % 2))) % ep_n

    barrier = pltpu.get_barrier_semaphore()

    def greet(i, _):
        pl.semaphore_signal(barrier, inc=1, device_id=(partner(i), own), device_id_type=MESH)
        return 0

    lax.fori_loop(0, ep_n - 1, greet, 0)
    for other in (
        (me, near),
        (me, far),
        (after // tp_n, after % tp_n),
        (before // tp_n, before % tp_n),
    ):
        pl.semaphore_signal(barrier, inc=1, device_id=other, device_id_type=MESH)

    def down_cols(c):
        return pl.ds(pl.multiple_of(c * part, LANES), part)

    loads = [
        pltpu.make_async_copy(
            rows_hbm.at[pl.ds(own * block_rows, block_rows)], mine_v, local_sem.at[0]
        ),
        pltpu.make_async_copy(pool_hbm, pool_v, local_sem.at[1]),
        pltpu.make_async_copy(wout_hbm, wout_v, local_sem.at[2]),
        pltpu.make_async_copy(gate_hbm.at[0], gate_all.at[0], local_sem.at[3]),
        pltpu.make_async_copy(up_hbm.at[0], up_all.at[0], local_sem.at[4]),
        pltpu.make_async_copy(wpool_hbm, wpool_ref, local_sem.at[5]),
    ]
    for load in loads:
        load.start()

    def own_down(c):
        return pltpu.make_async_copy(
            down_hbm.at[0, :, down_cols(c)], down_all.at[c, 0:local], local_sem.at[7 + c]
        )

    block = pl.ds(pl.multiple_of(own * block_rows, block_rows), block_rows)
    routes = routes_ref[:, block]
    weights = weight_ref[:, block]
    tall = max(ep_n, 16)
    expert_of = lax.broadcasted_iota(jnp.int32, (tall, block_rows), 0)
    names = [expert_of == routes[j : j + 1] for j in range(K)]
    named = jnp.where(names[0] | names[1], 1.0, 0.0).astype(BF16)
    earlier = (
        lax.broadcasted_iota(jnp.int32, (block_rows, block_rows), 0)
        < lax.broadcasted_iota(jnp.int32, (block_rows, block_rows), 1)
    )
    rank = dot(named, jnp.where(earlier, 1.0, 0.0).astype(BF16))
    slot_of = lax.broadcasted_iota(jnp.int32, (slots, block_rows), 0)
    spread = jnp.zeros((slots, block_rows), F32)
    merged = jnp.zeros((slots, block_rows), F32)
    for j in range(K):
        rank_j = jnp.sum(jnp.where(names[j], rank, 0.0), axis=0, keepdims=True)
        place = routes[j : j + 1] * cap + rank_j.astype(jnp.int32)
        hit = slot_of == place
        spread = spread + jnp.where(hit, 1.0, 0.0)
        merged = merged + jnp.where(hit, weights[j : j + 1], 0.0)
    spread = spread.astype(BF16)

    loads[0].wait()
    features = mine_v[...].astype(F32)
    inverse = lax.rsqrt(jnp.mean(features * features, axis=-1, keepdims=True) + EPS)
    normed_v[...] = (features * inverse * gain_ref[...]).astype(BF16)
    pl.semaphore_wait(barrier, ep_n + 3)

    def to_far(src, dst, at):
        return pltpu.make_async_remote_copy(
            src_ref=src,
            dst_ref=dst,
            send_sem=far_s.at[at],
            recv_sem=far_r.at[at],
            device_id=(me, far),
            device_id_type=MESH,
        )

    def to_near(src, dst, at, send, recv):
        return pltpu.make_async_remote_copy(
            src_ref=src,
            dst_ref=dst,
            send_sem=send.at[at],
            recv_sem=recv.at[at],
            device_id=(me, near),
            device_id_type=MESH,
        )

    def far_gate(k):
        some = pl.ds(k * deep, deep)
        return (
            to_far(gate_hbm.at[0, some], gate_all.at[2, some], 2 * k),
            to_far(up_hbm.at[0, some], up_all.at[2, some], 2 * k + 1),
        )

    def relay_gate(k):
        some = pl.ds(k * deep, deep)
        return (
            to_near(gate_all.at[2, some], gate_all.at[3, some], 2 * k, relay_s, relay_r),
            to_near(up_all.at[2, some], up_all.at[3, some], 2 * k + 1, relay_s, relay_r),
        )

    def far_down(c):
        return to_far(
            down_hbm.at[0, :, down_cols(c)],
            down_all.at[c, 2 * local : 3 * local],
            2 * gate_n + c,
        )

    def relay_down(c):
        return to_near(
            down_all.at[c, 2 * local : 3 * local],
            down_all.at[c, 3 * local : 4 * local],
            2 * gate_n + c,
            relay_s,
            relay_r,
        )

    def near_down(c):
        return to_near(
            down_hbm.at[0, :, down_cols(c)],
            down_all.at[c, local : 2 * local],
            2 + c,
            near_s,
            near_r,
        )

    near_gate = (
        to_near(gate_hbm.at[0], gate_all.at[1], 0, near_s, near_r),
        to_near(up_hbm.at[0], up_all.at[1], 1, near_s, near_r),
    )
    rows_here = pool_v.shape[0]
    halo = pltpu.make_async_remote_copy(
        src_ref=pool_hbm.at[rows_here - WMAX :],
        dst_ref=halo_v,
        send_sem=halo_s,
        recv_sem=halo_r,
        device_id=(after // tp_n, after % tp_n),
        device_id_type=MESH,
    )
    halo.start()
    for k in range(gate_n):
        for copy in far_gate(k):
            copy.start()

    def start_far_down(c, _):
        far_down(c).start()
        return 0

    lax.fori_loop(0, down_n, start_far_down, 0)

    step = 512

    def spread_cols(i, _):
        cols = pl.ds(pl.multiple_of(i * step, step), step)
        rows = dot(spread, normed_v[:, cols]).astype(BF16)
        outgoing[:, :, cols] = rows.reshape(ep_n, cap, step)
        return 0

    lax.fori_loop(0, width // step, spread_cols, 0)

    def go(peer, slot):
        return pltpu.make_async_remote_copy(
            src_ref=outgoing.at[peer],
            dst_ref=arrived.at[slot],
            send_sem=go_s.at[peer],
            recv_sem=go_r.at[slot],
            device_id=(peer, own),
            device_id_type=MESH,
        )

    def start_go(i, _):
        go(partner(i), me).start()
        return 0

    lax.fori_loop(0, ep_n - 1, start_go, 0)
    arrived[me] = outgoing[me]

    for copy in near_gate:
        copy.start()

    def start_near_down(c, _):
        near_down(c).start()
        own_down(c).start()
        return 0

    lax.fori_loop(0, down_n, start_near_down, 0)

    loads[1].wait()
    loads[5].wait()
    halo.wait_recv()
    position = (
        index * rows_here + lax.broadcasted_iota(jnp.int32, (rows_here, GDIM), 0)
    ).astype(F32)
    for g in range(wpool_ref.shape[0]):
        window = 2 ** (1 + g % 4)
        cols = slice(g * GDIM, (g + 1) * GDIM)
        head = jnp.where(index > 0, halo_v[:, cols].astype(F32), 0.0)
        here = pool_v[:, cols].astype(F32)
        running = jnp.concatenate([head, here], axis=0)
        shift = 1
        while shift < window:
            running = running + pltpu.roll(running, shift, 0)
            shift *= 2
        counted = jnp.minimum(position + 1.0, float(window))
        pooled = (running[WMAX:] / counted - here).astype(BF16)
        scaled_v[:, cols] = (dot(pooled, wpool_ref[g]) * scale_ref[:, cols]).astype(BF16)
    loads[2].wait()

    def mix_cols(i, _):
        cols = pl.ds(pl.multiple_of(i * step, step), step)
        mixer_v[:, cols] = dot(scaled_v[...], wout_v[:, cols]).astype(BF16)
        return 0

    lax.fori_loop(0, width // step, mix_cols, 0)
    def activate(slot, gate_val, up_val):
        value = gate_val / (1.0 + jnp.exp(-gate_val)) * up_val
        cols = pl.ds(pl.multiple_of(slot * local, LANES), local)
        hidden[:, cols] = value.astype(BF16)

    def relay(k):
        for copy in far_gate(k):
            copy.wait_recv()
        for copy in relay_gate(k):
            copy.start()

    for k in range(gate_n - 1):
        relay(k)
    loads[3].wait()
    loads[4].wait()
    for copy in near_gate:
        copy.wait_recv()

    def wait_go(i, _):
        go(me, partner(i)).wait_recv()
        return 0

    lax.fori_loop(0, ep_n - 1, wait_go, 0)

    def gated_slot(slot, _):
        rows = arrived[...].reshape(slots, width)
        activate(slot, dot(rows, gate_all[slot]), dot(rows, up_all[slot]))
        return 0

    lax.fori_loop(0, 2, gated_slot, 0)
    for k in range(gate_n - 1):
        for copy in relay_gate(k):
            copy.wait_recv()
    most = (gate_n - 1) * deep

    def most_slot(slot, _):
        rows = arrived[:, :, :most].reshape(slots, most)
        gate_sum[slot - 2] = dot(rows, gate_all[slot, :most])
        up_sum[slot - 2] = dot(rows, up_all[slot, :most])
        return 0

    lax.fori_loop(2, 4, most_slot, 0)
    relay(gate_n - 1)

    def last_slot(slot, _):
        @pl.when(slot == 3)
        def _():
            for copy in relay_gate(gate_n - 1):
                copy.wait_recv()

        rows = arrived[:, :, most:].reshape(slots, deep)
        activate(
            slot,
            gate_sum[slot - 2] + dot(rows, gate_all[slot, most:]),
            up_sum[slot - 2] + dot(rows, up_all[slot, most:]),
        )
        return 0

    lax.fori_loop(2, 4, last_slot, 0)

    def back(c, peer, slot):
        return pltpu.make_async_remote_copy(
            src_ref=result.at[c, peer],
            dst_ref=returned.at[c, slot],
            send_sem=back_s.at[c, peer],
            recv_sem=back_r.at[c, slot],
            device_id=(peer, own),
            device_id_type=MESH,
        )

    def down_part(c, _):
        far_down(c).wait_recv()
        relay_down(c).start()
        own_down(c).wait()
        near_down(c).wait_recv()
        relay_down(c).wait_recv()
        value = dot(hidden[...], down_all[c]).astype(BF16).reshape(ep_n, cap, part)
        result[c] = value

        def start_back(i, _):
            back(c, partner(i), me).start()
            return 0

        lax.fori_loop(0, ep_n - 1, start_back, 0)
        returned[c, me] = result[c, me]
        return 0

    lax.fori_loop(0, down_n, down_part, 0)

    merge = merged.T
    high = merge.astype(BF16)
    low = (merge - high.astype(F32)).astype(BF16)

    def combine(c, _):
        def wait_back(i, _):
            back(c, me, partner(i)).wait_recv()
            return 0

        lax.fori_loop(0, ep_n - 1, wait_back, 0)
        values = returned[c].reshape(slots, part)
        expert_v[:, down_cols(c)] = (dot(high, values) + dot(low, values)).astype(BF16)
        return 0

    lax.fori_loop(0, down_n, combine, 0)

    halo.wait_send()
    for k in range(gate_n):
        for copy in far_gate(k) + relay_gate(k):
            copy.wait_send()
    for copy in near_gate:
        copy.wait_send()

    def end_down(c, _):
        far_down(c).wait_send()
        relay_down(c).wait_send()
        near_down(c).wait_send()

        def end_back(i, _):
            back(c, partner(i), me).wait_send()
            return 0

        lax.fori_loop(0, ep_n - 1, end_back, 0)
        return 0

    lax.fori_loop(0, down_n, end_down, 0)

    def end_go(i, _):
        go(partner(i), me).wait_send()
        return 0

    lax.fori_loop(0, ep_n - 1, end_go, 0)


def on_device(
    pool_in,
    w_pool,
    pool_scale,
    w_out,
    expert_in,
    ffn_gain,
    routes,
    route_weight,
    w_gate,
    w_up,
    w_down,
):
    ep_n = lax.axis_size("ep")
    tp_n = lax.axis_size("tp")
    assert tp_n == 4 and w_gate.shape[0] == 1
    block_rows = routes.shape[0] // tp_n
    capacity = 3 * block_rows * K // (2 * ep_n)
    cap = -(-capacity // 16) * 16
    width = expert_in.shape[1]
    rows_here, pool_width = pool_in.shape
    local = w_gate.shape[2]
    slots = ep_n * cap
    down_n = 8
    part = width // down_n
    gate_n = 4
    vmem = pl.BlockSpec(memory_space=pltpu.VMEM)
    hbm = pl.BlockSpec(memory_space=pl.ANY)
    dma = pltpu.SemaphoreType.DMA
    return pl.pallas_call(
        functools.partial(kernel, (ep_n, tp_n, cap, gate_n, down_n)),
        out_shape=(
            pltpu.VMEM((rows_here, width), BF16),
            pltpu.VMEM((block_rows, width), BF16),
        ),
        in_specs=[vmem] * 4 + [hbm] * 7,
        out_specs=(vmem, vmem),
        scratch_shapes=[
            pltpu.VMEM(w_pool.shape, BF16),
            pltpu.VMEM((rows_here, pool_width), BF16),
            pltpu.VMEM((WMAX, pool_width), BF16),
            pltpu.VMEM((pool_width, width), BF16),
            pltpu.VMEM((rows_here, pool_width), BF16),
            pltpu.VMEM((block_rows, width), BF16),
            pltpu.VMEM((block_rows, width), BF16),
            pltpu.VMEM((ep_n, cap, width), BF16),
            pltpu.VMEM((ep_n, cap, width), BF16),
            pltpu.VMEM((tp_n, width, local), BF16),
            pltpu.VMEM((tp_n, width, local), BF16),
            pltpu.VMEM((2, slots, local), F32),
            pltpu.VMEM((2, slots, local), F32),
            pltpu.VMEM((slots, tp_n * local), BF16),
            pltpu.VMEM((down_n, tp_n * local, part), BF16),
            pltpu.VMEM((down_n, ep_n, cap, part), BF16),
            pltpu.VMEM((down_n, ep_n, cap, part), BF16),
            dma((7 + down_n,)),
            dma((2 * gate_n + down_n,)),
            dma((2 * gate_n + down_n,)),
            dma((2 + down_n,)),
            dma((2 + down_n,)),
            dma((2 * gate_n + down_n,)),
            dma((2 * gate_n + down_n,)),
            dma((ep_n,)),
            dma((ep_n,)),
            dma((down_n, ep_n)),
            dma((down_n, ep_n)),
            dma,
            dma,
        ],
        compiler_params=pltpu.CompilerParams(
            collective_id=0, has_side_effects=True, vmem_limit_bytes=60 * 1024 * 1024
        ),
    )(
        routes.T,
        route_weight.T,
        ffn_gain.reshape(1, -1),
        pool_scale.reshape(1, -1),
        w_pool,
        pool_in,
        w_out,
        expert_in,
        w_gate,
        w_up,
        w_down,
    )


def solution(mesh):
    placed = (
        P(("ep", "tp"), None),
        P(),
        P(),
        P(),
        P("ep", None),
        P(),
        P("ep", None),
        P("ep", None),
        P("ep", None, "tp"),
        P("ep", None, "tp"),
        P("ep", "tp", None),
    )
    return jax.shard_map(
        on_device,
        mesh=mesh,
        in_specs=placed,
        out_specs=(P(("ep", "tp"), None), P(("ep", "tp"), None)),
        check_vma=False,
    )
```

profile of v0, /device:TPU:0, one launch (start us, length us, event | category | flops | bytes accessed | tf_op | source)
XLA Modules:
  0.0 99.4 jit_solution(1339012405160748886)
XLA Ops:
  0.6 97.0 %shard_map.122 = (bf16[256,2048]{1,0:T(8,128)(2,1)S(1)}, bf16[128,2048]{1,0:T(8,128)(2,1)S(1)}) custom-call(s32[2,512]{1,0:T(2,128)} %bitcast.5, f32[2,512]{1,0:T(2,128)} %bitcast.6, f32[1,2048]{1,0:T(1,128)} %bitcast.4, f32[1,1024]{1,0:T(1,128)} %bitcast.7, bf16[8,128,128]{2,1,0:T(8,128)(2,1)} %wpool_hbm.1, bf16[256,1024]{1,0:T(8,128)(2,1)} %pool_hbm.1, ...), custom_call_target="tpu_custom_call" | custom-call | tf_op jit(solution)/shard_map/pallas_call | solution.py:462
  97.7 1.0 copy.15
  98.6 0.8 copy.16
where the time goes:
time: 99.6 us; the launch traced here: 99.4 us
  Pallas kernels  97 us (97%)
  local copies, waits for them, and re-layouts  1.77 us (2%)
    pallas_call x1, Pallas kernels, on_device(): pl.pallas_call(functools.partial(kernel, (ep_n, tp_n, cap, gate_n, down_n...  97 us

commit v1 on v0

--- a/solution.py
+++ b/solution.py
@@ -53,6 +53,13 @@
     down_all,
     result,
     returned,
+    relay_in,
+    relay_out,
+    dense,
+    near_routes,
+    near_weights,
+    merge_high,
+    merge_low,
     local_sem,
     far_s,
     far_r,
@@ -64,6 +71,11 @@
     go_r,
     back_s,
     back_r,
+    group_r,
+    dense_s,
+    dense_r,
+    names_s,
+    names_r,
     halo_s,
     halo_r,
 ):
@@ -82,6 +94,17 @@
     deep = width // gate_n
     part = width // down_n
 
+    half = ep_n // 2
+    plane = ep_n // 4
+    upper = me // half
+    first = upper * half
+    other = half - first
+    mine = me - first
+    relays = half - plane + upper * plane
+    is_relay = (me >= half - plane) & (me < half + plane)
+    my_relay = half - upper * plane + me % plane
+    my_turn = mine // plane
+
     def partner(i):
         return (me + ep_n // 2 + ((i + 1) // 2) * (1 - 2 * (i % 2))) % ep_n
 
@@ -92,13 +115,13 @@
         return 0
 
     lax.fori_loop(0, ep_n - 1, greet, 0)
-    for other in (
+    for there in (
         (me, near),
         (me, far),
         (after // tp_n, after % tp_n),
         (before // tp_n, before % tp_n),
     ):
-        pl.semaphore_signal(barrier, inc=1, device_id=other, device_id_type=MESH)
+        pl.semaphore_signal(barrier, inc=1, device_id=there, device_id_type=MESH)
 
     def down_cols(c):
         return pl.ds(pl.multiple_of(c * part, LANES), part)
@@ -121,33 +144,6 @@
             down_hbm.at[0, :, down_cols(c)], down_all.at[c, 0:local], local_sem.at[7 + c]
         )
 
-    block = pl.ds(pl.multiple_of(own * block_rows, block_rows), block_rows)
-    routes = routes_ref[:, block]
-    weights = weight_ref[:, block]
-    tall = max(ep_n, 16)
-    expert_of = lax.broadcasted_iota(jnp.int32, (tall, block_rows), 0)
-    names = [expert_of == routes[j : j + 1] for j in range(K)]
-    named = jnp.where(names[0] | names[1], 1.0, 0.0).astype(BF16)
-    earlier = (
-        lax.broadcasted_iota(jnp.int32, (block_rows, block_rows), 0)
-        < lax.broadcasted_iota(jnp.int32, (block_rows, block_rows), 1)
-    )
-    rank = dot(named, jnp.where(earlier, 1.0, 0.0).astype(BF16))
-    slot_of = lax.broadcasted_iota(jnp.int32, (slots, block_rows), 0)
-    spread = jnp.zeros((slots, block_rows), F32)
-    merged = jnp.zeros((slots, block_rows), F32)
-    for j in range(K):
-        rank_j = jnp.sum(jnp.where(names[j], rank, 0.0), axis=0, keepdims=True)
-        place = routes[j : j + 1] * cap + rank_j.astype(jnp.int32)
-        hit = slot_of == place
-        spread = spread + jnp.where(hit, 1.0, 0.0)
-        merged = merged + jnp.where(hit, weights[j : j + 1], 0.0)
-    spread = spread.astype(BF16)
-
-    loads[0].wait()
-    features = mine_v[...].astype(F32)
-    inverse = lax.rsqrt(jnp.mean(features * features, axis=-1, keepdims=True) + EPS)
-    normed_v[...] = (features * inverse * gain_ref[...]).astype(BF16)
     pl.semaphore_wait(barrier, ep_n + 3)
 
     def to_far(src, dst, at):
@@ -223,6 +219,19 @@
         device_id_type=MESH,
     )
     halo.start()
+
+    def to_relay(src, dst, at):
+        return pltpu.make_async_remote_copy(
+            src_ref=src.at[:, pl.ds(pl.multiple_of(own * block_rows, block_rows), block_rows)],
+            dst_ref=dst,
+            send_sem=names_s.at[at],
+            recv_sem=names_r.at[at, my_turn],
+            device_id=(my_relay, own),
+            device_id_type=MESH,
+        )
+
+    to_relay(routes_ref, near_routes.at[my_turn], 0).start()
+    to_relay(weight_ref, near_weights.at[my_turn], 1).start()
     for k in range(gate_n):
         for copy in far_gate(k):
             copy.start()
@@ -232,6 +241,47 @@
         return 0
 
     lax.fori_loop(0, down_n, start_far_down, 0)
+
+    block = pl.ds(pl.multiple_of(own * block_rows, block_rows), block_rows)
+    tall = max(ep_n, 16)
+    expert_of = lax.broadcasted_iota(jnp.int32, (tall, block_rows), 0)
+    earlier = (
+        lax.broadcasted_iota(jnp.int32, (block_rows, block_rows), 0)
+        < lax.broadcasted_iota(jnp.int32, (block_rows, block_rows), 1)
+    )
+    earlier = jnp.where(earlier, 1.0, 0.0).astype(BF16)
+
+    def places(routes):
+        names = [expert_of == routes[j : j + 1] for j in range(K)]
+        named = jnp.where(names[0] | names[1], 1.0, 0.0).astype(BF16)
+        rank = dot(named, earlier)
+        return [
+            routes[j : j + 1] * cap
+            + jnp.sum(jnp.where(names[j], rank, 0.0), axis=0, keepdims=True).astype(jnp.int32)
+            for j in range(K)
+        ]
+
+    def set_merge(at, place, weights):
+        slot_of = first * cap + lax.broadcasted_iota(jnp.int32, (half * cap, block_rows), 0)
+        merged = jnp.zeros((half * cap, block_rows), F32)
+        for j in range(K):
+            merged = merged + jnp.where(slot_of == place[j], weights[j : j + 1], 0.0)
+        merge = merged.T
+        high = merge.astype(BF16)
+        merge_high[at] = high
+        merge_low[at] = (merge - high.astype(F32)).astype(BF16)
+
+    place = places(routes_ref[:, block])
+    slot_of = lax.broadcasted_iota(jnp.int32, (slots, block_rows), 0)
+    spread = jnp.zeros((slots, block_rows), F32)
+    for j in range(K):
+        spread = spread + jnp.where(slot_of == place[j], 1.0, 0.0)
+    spread = spread.astype(BF16)
+
+    loads[0].wait()
+    features = mine_v[...].astype(F32)
+    inverse = lax.rsqrt(jnp.mean(features * features, axis=-1, keepdims=True) + EPS)
+    normed_v[...] = (features * inverse * gain_ref[...]).astype(BF16)
 
     step = 512
 
@@ -269,6 +319,8 @@
         return 0
 
     lax.fori_loop(0, down_n, start_near_down, 0)
+
+    set_merge(0, place, weight_ref[:, block])
 
     loads[1].wait()
     loads[5].wait()
@@ -297,6 +349,21 @@
         return 0
 
     lax.fori_loop(0, width // step, mix_cols, 0)
+
+    @pl.when(is_relay)
+    def _():
+        for k in range(2):
+            for at, held in enumerate((near_routes, near_weights)):
+                pltpu.make_async_remote_copy(
+                    src_ref=held.at[k],
+                    dst_ref=held.at[k],
+                    send_sem=names_s.at[at],
+                    recv_sem=names_r.at[at, k],
+                    device_id=(my_relay, own),
+                    device_id_type=MESH,
+                ).wait_recv()
+            set_merge(1 + k, places(near_routes[k]), near_weights[k])
+
     def activate(slot, gate_val, up_val):
         value = gate_val / (1.0 + jnp.exp(-gate_val)) * up_val
         cols = pl.ds(pl.multiple_of(slot * local, LANES), local)
@@ -357,15 +424,53 @@
 
     lax.fori_loop(2, 4, last_slot, 0)
 
+    def peer_of(i):
+        return (mine + 1 + i) % half
+
     def back(c, peer, slot):
         return pltpu.make_async_remote_copy(
-            src_ref=result.at[c, peer],
+            src_ref=result.at[c, first + peer],
             dst_ref=returned.at[c, slot],
-            send_sem=back_s.at[c, peer],
+            send_sem=back_s.at[c, first + peer],
             recv_sem=back_r.at[c, slot],
-            device_id=(peer, own),
+            device_id=(first + peer, own),
             device_id_type=MESH,
         )
+
+    def group(c, i, slot):
+        return pltpu.make_async_remote_copy(
+            src_ref=result.at[c, other + i],
+            dst_ref=relay_in.at[c, i // plane, slot],
+            send_sem=back_s.at[c, other + i],
+            recv_sem=group_r.at[c, i // plane, slot],
+            device_id=(relays + i % plane, own),
+            device_id_type=MESH,
+        )
+
+    def dense_to(c, k):
+        return pltpu.make_async_remote_copy(
+            src_ref=relay_out.at[c, k],
+            dst_ref=dense.at[c],
+            send_sem=dense_s.at[c, k],
+            recv_sem=dense_r.at[c],
+            device_id=(other + k * plane + me % plane, own),
+            device_id_type=MESH,
+        )
+
+    def weighed(at, values):
+        return dot(merge_high[at], values) + dot(merge_low[at], values)
+
+    def pass_on(c):
+        for k in range(2):
+
+            def wait_group(i, _):
+                group(c, k * plane + me % plane, peer_of(i)).wait_recv()
+                return 0
+
+            lax.fori_loop(0, half - 1, wait_group, 0)
+            values = relay_in[c, k].reshape(half * cap, part)
+            relay_out[c, k] = weighed(1 + k, values).astype(BF16)
+            dense_to(c, k).start()
 
     def down_part(c, _):
         far_down(c).wait_recv()
@@ -376,33 +481,62 @@
         value = dot(hidden[...], down_all[c]).astype(BF16).reshape(ep_n, cap, part)
         result[c] = value
 
+        def start_group(i, _):
+            @pl.when(relays + i % plane != me)
+            def _():
+                group(c, i, mine).start()
+
+            return 0
+
+        lax.fori_loop(0, half, start_group, 0)
+
         def start_back(i, _):
-            back(c, partner(i), me).start()
+            back(c, peer_of(i), mine).start()
             return 0
 
-        lax.fori_loop(0, ep_n - 1, start_back, 0)
-        returned[c, me] = result[c, me]
+        lax.fori_loop(0, half - 1, start_back, 0)
+        returned[c, mine] = result[c, me]
+
+        @pl.when(is_relay)
+        def _():
+            for k in range(2):
+                relay_in[c, k, mine] = result[c, other + k * plane + me % plane]
+
+            @pl.when(c > 0)
+            def _():
+                pass_on(c - 1)
+
         return 0
 
     lax.fori_loop(0, down_n, down_part, 0)
 
-    merge = merged.T
-    high = merge.astype(BF16)
-    low = (merge - high.astype(F32)).astype(BF16)
+    @pl.when(is_relay)
+    def _():
+        pass_on(down_n - 1)
 
     def combine(c, _):
         def wait_back(i, _):
-            back(c, me, partner(i)).wait_recv()
+            back(c, mine, peer_of(i)).wait_recv()
             return 0
 
-        lax.fori_loop(0, ep_n - 1, wait_back, 0)
-        values = returned[c].reshape(slots, part)
-        expert_v[:, down_cols(c)] = (dot(high, values) + dot(low, values)).astype(BF16)
+        lax.fori_loop(0, half - 1, wait_back, 0)
+        pltpu.make_async_remote_copy(
+            src_ref=dense.at[c],
+            dst_ref=dense.at[c],
+            send_sem=dense_s.at[c, 0],
+            recv_sem=dense_r.at[c],
+            device_id=(my_relay, own),
+            device_id_type=MESH,
+        ).wait_recv()
+        values = returned[c].reshape(half * cap, part)
+        expert_v[:, down_cols(c)] = (weighed(0, values) + dense[c].astype(F32)).astype(BF16)
         return 0
 
     lax.fori_loop(0, down_n, combine, 0)
 
     halo.wait_send()
+    to_relay(routes_ref, near_routes.at[my_turn], 0).wait_send()
+    to_relay(weight_ref, near_weights.at[my_turn], 1).wait_send()
     for k in range(gate_n):
         for copy in far_gate(k) + relay_gate(k):
             copy.wait_send()
@@ -415,10 +549,25 @@
         near_down(c).wait_send()
 
         def end_back(i, _):
-            back(c, partner(i), me).wait_send()
+            back(c, peer_of(i), mine).wait_send()
             return 0
 
-        lax.fori_loop(0, ep_n - 1, end_back, 0)
+        lax.fori_loop(0, half - 1, end_back, 0)
+
+        def end_group(i, _):
+            @pl.when(relays + i % plane != me)
+            def _():
+                group(c, i, mine).wait_send()
+
+            return 0
+
+        lax.fori_loop(0, half, end_group, 0)
+
+        @pl.when(is_relay)
+        def _():
+            for k in range(2):
+                dense_to(c, k).wait_send()
+
         return 0
 
     lax.fori_loop(0, down_n, end_down, 0)
@@ -445,7 +594,8 @@
 ):
     ep_n = lax.axis_size("ep")
     tp_n = lax.axis_size("tp")
-    assert tp_n == 4 and w_gate.shape[0] == 1
+    assert tp_n == 4 and ep_n % 4 == 0 and w_gate.shape[0] == 1
+    half = ep_n // 2
     block_rows = routes.shape[0] // tp_n
     capacity = 3 * block_rows * K // (2 * ep_n)
     cap = -(-capacity // 16) * 16
@@ -484,7 +634,14 @@
             pltpu.VMEM((slots, tp_n * local), BF16),
             pltpu.VMEM((down_n, tp_n * local, part), BF16),
             pltpu.VMEM((down_n, ep_n, cap, part), BF16),
-            pltpu.VMEM((down_n, ep_n, cap, part), BF16),
+            pltpu.VMEM((down_n, half, cap, part), BF16),
+            pltpu.VMEM((down_n, 2, half, cap, part), BF16),
+            pltpu.VMEM((down_n, 2, block_rows, part), BF16),
+            pltpu.VMEM((down_n, block_rows, part), BF16),
+            pltpu.VMEM((2, K, block_rows), jnp.int32),
+            pltpu.VMEM((2, K, block_rows), F32),
+            pltpu.VMEM((3, block_rows, half * cap), BF16),
+            pltpu.VMEM((3, block_rows, half * cap), BF16),
             dma((7 + down_n,)),
             dma((2 * gate_n + down_n,)),
             dma((2 * gate_n + down_n,)),
@@ -495,7 +652,12 @@
             dma((ep_n,)),
             dma((ep_n,)),
             dma((down_n, ep_n)),
-            dma((down_n, ep_n)),
+            dma((down_n, half)),
+            dma((down_n, 2, half)),
+            dma((down_n, 2)),
+            dma((down_n,)),
+            dma((2,)),
+            dma((2, 2)),
             dma,
             dma,
         ],

time: 99.6 us -> 94.6 us (0.950)
  Pallas kernels: 97 us -> 92 us
    pallas_call x1, Pallas kernels: 97 us -> 92 us  [on_device(): pl.pallas_call(functools.partial(kernel, (ep_n, tp_n, cap, gate_n, down_n...]
where the time goes in v1:
time: 94.6 us; the launch traced here: 94.4 us
  Pallas kernels  92 us (97%)
  local copies, waits for them, and re-layouts  1.77 us (2%)
    pallas_call x1, Pallas kernels, on_device(): pl.pallas_call(functools.partial(kernel, (ep_n, tp_n, cap, gate_n, down_n...  92 us

profile of v1, /device:TPU:0, one launch (start us, length us, event | category | flops | bytes accessed | tf_op | source)
XLA Modules:
  0.0 94.4 jit_solution(7986745698502576724)
XLA Ops:
  0.6 92.0 %shard_map.122 = (bf16[256,2048]{1,0:T(8,128)(2,1)S(1)}, bf16[128,2048]{1,0:T(8,128)(2,1)S(1)}) custom-call(s32[2,512]{1,0:T(2,128)} %bitcast.5, f32[2,512]{1,0:T(2,128)} %bitcast.6, f32[1,2048]{1,0:T(1,128)} %bitcast.4, f32[1,1024]{1,0:T(1,128)} %bitcast.7, bf16[8,128,128]{2,1,0:T(8,128)(2,1)} %wpool_hbm.1, bf16[256,1024]{1,0:T(8,128)(2,1)} %pool_hbm.1, ...), custom_call_target="tpu_custom_call" | custom-call | tf_op jit(solution)/shard_map/pallas_call | solution.py:612
  92.6 1.0 %copy.15 = bf16[256,2048]{1,0:T(8,128)(2,1)} copy(bf16[256,2048]{1,0:T(8,128)(2,1)S(1)} %get-tuple-element.2) | data formatting | bytes 2097152
  93.6 0.8 copy.16

commit v2 on v1

--- a/solution.py
+++ b/solution.py
@@ -78,6 +78,8 @@
     names_r,
     halo_s,
     halo_r,
+    hello,
+    ready,
 ):
     ep_n, tp_n, cap, gate_n, down_n = dims
     me = lax.axis_index("ep")
@@ -110,18 +112,12 @@
 
     barrier = pltpu.get_barrier_semaphore()
 
-    def greet(i, _):
-        pl.semaphore_signal(barrier, inc=1, device_id=(partner(i), own), device_id_type=MESH)
-        return 0
-
-    lax.fori_loop(0, ep_n - 1, greet, 0)
-    for there in (
-        (me, near),
-        (me, far),
-        (after // tp_n, after % tp_n),
-        (before // tp_n, before % tp_n),
-    ):
-        pl.semaphore_signal(barrier, inc=1, device_id=there, device_id_type=MESH)
+    lead = own < tp_n // 2
+    follow = own >= tp_n // 2
+
+    @pl.when(lead)
+    def _():
+        pl.semaphore_signal(barrier, inc=1, device_id=(me, far), device_id_type=MESH)
 
     def down_cols(c):
         return pl.ds(pl.multiple_of(c * part, LANES), part)
@@ -144,7 +140,14 @@
             down_hbm.at[0, :, down_cols(c)], down_all.at[c, 0:local], local_sem.at[7 + c]
         )
 
-    pl.semaphore_wait(barrier, ep_n + 3)
+    @pl.when(follow)
+    def _():
+        pl.semaphore_wait(barrier, 1)
+        pl.semaphore_signal(hello, inc=1, device_id=(me, far), device_id_type=MESH)
+
+    @pl.when(lead)
+    def _():
+        pl.semaphore_wait(hello, 1)
 
     def to_far(src, dst, at):
         return pltpu.make_async_remote_copy(
@@ -218,7 +221,6 @@
         device_id=(after // tp_n, after % tp_n),
         device_id_type=MESH,
     )
-    halo.start()
 
     def to_relay(src, dst, at):
         return pltpu.make_async_remote_copy(
@@ -230,17 +232,27 @@
             device_id_type=MESH,
         )
 
-    to_relay(routes_ref, near_routes.at[my_turn], 0).start()
-    to_relay(weight_ref, near_weights.at[my_turn], 1).start()
-    for k in range(gate_n):
-        for copy in far_gate(k):
+    ahead = [copy for k in range(gate_n) for copy in far_gate(k)]
+    for copy in ahead[:3]:
+        copy.start()
+
+    @pl.when(follow)
+    def _():
+        for copy in ahead[3:4]:
             copy.start()
 
-    def start_far_down(c, _):
-        far_down(c).start()
-        return 0
-
-    lax.fori_loop(0, down_n, start_far_down, 0)
+    @pl.when(lead)
+    def _():
+        def greet(i, _):
+            peer = (me + 1 + i) % ep_n
+            pl.semaphore_signal(barrier, inc=1, device_id=(peer, own), device_id_type=MESH)
+            return 0
+
+        lax.fori_loop(0, ep_n - 1, greet, 0)
+        beside = (me + ep_n - 1 + 2 * (own % 2)) % ep_n
+        for there in ((me, near), (beside, near)):
+            pl.semaphore_signal(barrier, inc=1, device_id=there, device_id_type=MESH)
+
 
     block = pl.ds(pl.multiple_of(own * block_rows, block_rows), block_rows)
     tall = max(ep_n, 16)
@@ -278,12 +290,40 @@
         spread = spread + jnp.where(slot_of == place[j], 1.0, 0.0)
     spread = spread.astype(BF16)
 
+    @pl.when(lead)
+    def _():
+        pl.semaphore_wait(barrier, ep_n + 1)
+        pl.semaphore_signal(ready, inc=1, device_id=(me, far), device_id_type=MESH)
+
+    @pl.when(follow)
+    def _():
+        pl.semaphore_wait(ready, 1)
+
+    halo.start()
+
+    @pl.when(lead)
+    def _():
+        for copy in ahead[3:4]:
+            copy.start()
+
+    for copy in ahead[4:]:
+        copy.start()
+
+    def start_far_down(c, _):
+        far_down(c).start()
+        return 0
+
+    lax.fori_loop(0, down_n, start_far_down, 0)
+    to_relay(routes_ref, near_routes.at[my_turn], 0).start()
+    to_relay(weight_ref, near_weights.at[my_turn], 1).start()
+
     loads[0].wait()
     features = mine_v[...].astype(F32)
     inverse = lax.rsqrt(jnp.mean(features * features, axis=-1, keepdims=True) + EPS)
     normed_v[...] = (features * inverse * gain_ref[...]).astype(BF16)
 
     step = 512
+    lag = 2
 
     def spread_cols(i, _):
         cols = pl.ds(pl.multiple_of(i * step, step), step)
@@ -502,9 +542,9 @@
             for k in range(2):
                 relay_in[c, k, mine] = result[c, other + k * plane + me % plane]
 
-            @pl.when(c > 0)
+            @pl.when(c >= lag)
             def _():
-                pass_on(c - 1)
+                pass_on(c - lag)
 
         return 0
 
@@ -512,7 +552,11 @@
 
     @pl.when(is_relay)
     def _():
-        pass_on(down_n - 1)
+        def pass_rest(c, _):
+            pass_on(c)
+            return 0
+
+        lax.fori_loop(down_n - lag, down_n, pass_rest, 0)
 
     def combine(c, _):
         def wait_back(i, _):
@@ -605,7 +649,7 @@
     slots = ep_n * cap
     down_n = 8
     part = width // down_n
-    gate_n = 4
+    gate_n = 8
     vmem = pl.BlockSpec(memory_space=pltpu.VMEM)
     hbm = pl.BlockSpec(memory_space=pl.ANY)
     dma = pltpu.SemaphoreType.DMA
@@ -660,6 +704,8 @@
             dma((2, 2)),
             dma,
             dma,
+            pltpu.SemaphoreType.REGULAR,
+            pltpu.SemaphoreType.REGULAR,
         ],
         compiler_params=pltpu.CompilerParams(
             collective_id=0, has_side_effects=True, vmem_limit_bytes=60 * 1024 * 1024

time: 94.6 us -> 93.2 us (0.985)
  Pallas kernels: 92 us -> 90.6 us
    pallas_call x1, Pallas kernels: 92 us -> 90.6 us  [on_device(): pl.pallas_call(functools.partial(kernel, (ep_n, tp_n, cap, gate_n, down_n...]
where the time goes in v2:
time: 93.2 us; the launch traced here: 93 us
  Pallas kernels  90.6 us (97%)
  local copies, waits for them, and re-layouts  1.77 us (2%)
    pallas_call x1, Pallas kernels, on_device(): pl.pallas_call(functools.partial(kernel, (ep_n, tp_n, cap, gate_n, down_n...  90.6 us

profile of v2, /device:TPU:0, one launch (start us, length us, event | category | flops | bytes accessed | tf_op | source)
XLA Modules:
  0.0 93.0 jit_solution(1148730628202437871)
XLA Ops:
  0.6 90.6 %shard_map.122 = (bf16[256,2048]{1,0:T(8,128)(2,1)S(1)}, bf16[128,2048]{1,0:T(8,128)(2,1)S(1)}) custom-call(s32[2,512]{1,0:T(2,128)} %bitcast.5, f32[2,512]{1,0:T(2,128)} %bitcast.6, f32[1,2048]{1,0:T(1,128)} %bitcast.4, f32[1,1024]{1,0:T(1,128)} %bitcast.7, bf16[8,128,128]{2,1,0:T(8,128)(2,1)} %wpool_hbm.1, bf16[256,1024]{1,0:T(8,128)(2,1)} %pool_hbm.1, ...), custom_call_target="tpu_custom_call" | custom-call | tf_op jit(solution)/shard_map/pallas_call | solution.py:656
  91.2 1.0 %copy.15 = bf16[256,2048]{1,0:T(8,128)(2,1)} copy(bf16[256,2048]{1,0:T(8,128)(2,1)S(1)} %get-tuple-element.2) | data formatting | bytes 2097152
  92.2 0.8 copy.16

commit v3 on v2

--- a/solution.py
+++ b/solution.py
@@ -81,7 +81,9 @@
     hello,
     ready,
 ):
-    ep_n, tp_n, cap, gate_n, down_n = dims
+    ep_n, tp_n, cap, gate_n, sizes = dims
+    down_n = len(sizes)
+    starts = [sum(sizes[:c]) for c in range(down_n)]
     me = lax.axis_index("ep")
     own = lax.axis_index("tp")
     near = own + 1 - 2 * (own % 2)
@@ -94,7 +96,6 @@
     slots = ep_n * cap
     local = gate_hbm.shape[2]
     deep = width // gate_n
-    part = width // down_n
 
     half = ep_n // 2
     plane = ep_n // 4
@@ -120,7 +121,7 @@
         pl.semaphore_signal(barrier, inc=1, device_id=(me, far), device_id_type=MESH)
 
     def down_cols(c):
-        return pl.ds(pl.multiple_of(c * part, LANES), part)
+        return pl.ds(starts[c], sizes[c])
 
     loads = [
         pltpu.make_async_copy(
@@ -132,13 +133,17 @@
         pltpu.make_async_copy(up_hbm.at[0], up_all.at[0], local_sem.at[4]),
         pltpu.make_async_copy(wpool_hbm, wpool_ref, local_sem.at[5]),
     ]
-    for load in loads:
-        load.start()
+    for i in (3, 4, 0, 1, 5):
+        loads[i].start()
 
     def own_down(c):
         return pltpu.make_async_copy(
-            down_hbm.at[0, :, down_cols(c)], down_all.at[c, 0:local], local_sem.at[7 + c]
-        )
+            down_hbm.at[0, :, down_cols(c)], down_all.at[0:local, down_cols(c)], local_sem.at[7 + c]
+        )
+
+    for c in range(down_n):
+        own_down(c).start()
+    loads[2].start()
 
     @pl.when(follow)
     def _():
@@ -186,14 +191,14 @@
     def far_down(c):
         return to_far(
             down_hbm.at[0, :, down_cols(c)],
-            down_all.at[c, 2 * local : 3 * local],
+            down_all.at[2 * local : 3 * local, down_cols(c)],
             2 * gate_n + c,
         )
 
     def relay_down(c):
         return to_near(
-            down_all.at[c, 2 * local : 3 * local],
-            down_all.at[c, 3 * local : 4 * local],
+            down_all.at[2 * local : 3 * local, down_cols(c)],
+            down_all.at[3 * local : 4 * local, down_cols(c)],
             2 * gate_n + c,
             relay_s,
             relay_r,
@@ -201,16 +206,16 @@
 
     def near_down(c):
         return to_near(
-            down_hbm.at[0, :, down_cols(c)],
-            down_all.at[c, local : 2 * local],
+            down_all.at[0:local, down_cols(c)],
+            down_all.at[local : 2 * local, down_cols(c)],
             2 + c,
             near_s,
             near_r,
         )
 
     near_gate = (
-        to_near(gate_hbm.at[0], gate_all.at[1], 0, near_s, near_r),
-        to_near(up_hbm.at[0], up_all.at[1], 1, near_s, near_r),
+        to_near(gate_all.at[0], gate_all.at[1], 0, near_s, near_r),
+        to_near(up_all.at[0], up_all.at[1], 1, near_s, near_r),
     )
     rows_here = pool_v.shape[0]
     halo = pltpu.make_async_remote_copy(
@@ -313,7 +318,9 @@
         far_down(c).start()
         return 0
 
-    lax.fori_loop(0, down_n, start_far_down, 0)
+    for c in range(down_n):
+        own_down(c).wait()
+        start_far_down(c, 0)
     to_relay(routes_ref, near_routes.at[my_turn], 0).start()
     to_relay(weight_ref, near_weights.at[my_turn], 1).start()
 
@@ -324,6 +331,7 @@
 
     step = 512
     lag = 2
+    late = 2
 
     def spread_cols(i, _):
         cols = pl.ds(pl.multiple_of(i * step, step), step)
@@ -350,15 +358,17 @@
     lax.fori_loop(0, ep_n - 1, start_go, 0)
     arrived[me] = outgoing[me]
 
+    loads[3].wait()
+    loads[4].wait()
     for copy in near_gate:
         copy.start()
 
     def start_near_down(c, _):
         near_down(c).start()
-        own_down(c).start()
-        return 0
-
-    lax.fori_loop(0, down_n, start_near_down, 0)
+        return 0
+
+    for c in range(down_n):
+        start_near_down(c, 0)
 
     set_merge(0, place, weight_ref[:, block])
 
@@ -417,8 +427,6 @@
 
     for k in range(gate_n - 1):
         relay(k)
-    loads[3].wait()
-    loads[4].wait()
     for copy in near_gate:
         copy.wait_recv()
 
@@ -469,8 +477,8 @@
 
     def back(c, peer, slot):
         return pltpu.make_async_remote_copy(
-            src_ref=result.at[c, first + peer],
-            dst_ref=returned.at[c, slot],
+            src_ref=result.at[first + peer, :, down_cols(c)],
+            dst_ref=returned.at[slot, :, down_cols(c)],
             send_sem=back_s.at[c, first + peer],
             recv_sem=back_r.at[c, slot],
             device_id=(first + peer, own),
@@ -479,8 +487,8 @@
 
     def group(c, i, slot):
         return pltpu.make_async_remote_copy(
-            src_ref=result.at[c, other + i],
-            dst_ref=relay_in.at[c, i // plane, slot],
+            src_ref=result.at[other + i, :, down_cols(c)],
+            dst_ref=relay_in.at[i // plane, slot, :, down_cols(c)],
             send_sem=back_s.at[c, other + i],
             recv_sem=group_r.at[c, i // plane, slot],
             device_id=(relays + i % plane, own),
@@ -489,8 +497,8 @@
 
     def dense_to(c, k):
         return pltpu.make_async_remote_copy(
-            src_ref=relay_out.at[c, k],
-            dst_ref=dense.at[c],
+            src_ref=relay_out.at[k, :, down_cols(c)],
+            dst_ref=dense.at[:, down_cols(c)],
             send_sem=dense_s.at[c, k],
             recv_sem=dense_r.at[c],
             device_id=(other + k * plane + me % plane, own),
@@ -508,18 +516,24 @@
                 return 0
 
             lax.fori_loop(0, half - 1, wait_group, 0)
-            values = relay_in[c, k].reshape(half * cap, part)
-            relay_out[c, k] = weighed(1 + k, values).astype(BF16)
+            values = relay_in[k, :, :, down_cols(c)].reshape(half * cap, sizes[c])
+            relay_out[k, :, down_cols(c)] = weighed(1 + k, values).astype(BF16)
             dense_to(c, k).start()
+
+    def start_backs(c):
+        def start_back(i, _):
+            back(c, peer_of(i), mine).start()
+            return 0
+
+        lax.fori_loop(0, half - 1, start_back, 0)
 
     def down_part(c, _):
         far_down(c).wait_recv()
         relay_down(c).start()
-        own_down(c).wait()
         near_down(c).wait_recv()
         relay_down(c).wait_recv()
-        value = dot(hidden[...], down_all[c]).astype(BF16).reshape(ep_n, cap, part)
-        result[c] = value
+        value = dot(hidden[...], down_all[:, down_cols(c)]).astype(BF16)
+        result[:, :, down_cols(c)] = value.reshape(ep_n, cap, sizes[c])
 
         def start_group(i, _):
             @pl.when(relays + i % plane != me)
@@ -530,33 +544,30 @@
 
         lax.fori_loop(0, half, start_group, 0)
 
-        def start_back(i, _):
-            back(c, peer_of(i), mine).start()
-            return 0
-
-        lax.fori_loop(0, half - 1, start_back, 0)
-        returned[c, mine] = result[c, me]
+        if c >= late:
+            start_backs(c - late)
+        returned[mine, :, down_cols(c)] = result[me, :, down_cols(c)]
 
         @pl.when(is_relay)
         def _():
             for k in range(2):
-                relay_in[c, k, mine] = result[c, other + k * plane + me % plane]
-
-            @pl.when(c >= lag)
-            def _():
+                far_rows = result[other + k * plane + me % plane, :, down_cols(c)]
+                relay_in[k, mine, :, down_cols(c)] = far_rows
+
+            if c >= lag:
                 pass_on(c - lag)
 
         return 0
 
-    lax.fori_loop(0, down_n, down_part, 0)
+    for c in range(down_n):
+        down_part(c, 0)
+    for c in range(down_n - late, down_n):
+        start_backs(c)
 
     @pl.when(is_relay)
     def _():
-        def pass_rest(c, _):
+        for c in range(down_n - lag, down_n):
             pass_on(c)
-            return 0
-
-        lax.fori_loop(down_n - lag, down_n, pass_rest, 0)
 
     def combine(c, _):
         def wait_back(i, _):
@@ -565,18 +576,20 @@
 
         lax.fori_loop(0, half - 1, wait_back, 0)
         pltpu.make_async_remote_copy(
-            src_ref=dense.at[c],
-            dst_ref=dense.at[c],
+            src_ref=dense.at[:, down_cols(c)],
+            dst_ref=dense.at[:, down_cols(c)],
             send_sem=dense_s.at[c, 0],
             recv_sem=dense_r.at[c],
             device_id=(my_relay, own),
             device_id_type=MESH,
         ).wait_recv()
-        values = returned[c].reshape(half * cap, part)
-        expert_v[:, down_cols(c)] = (weighed(0, values) + dense[c].astype(F32)).astype(BF16)
-        return 0
-
-    lax.fori_loop(0, down_n, combine, 0)
+        values = returned[:, :, down_cols(c)].reshape(half * cap, sizes[c])
+        total_val = weighed(0, values) + dense[:, down_cols(c)].astype(F32)
+        expert_v[:, down_cols(c)] = total_val.astype(BF16)
+        return 0
+
+    for c in range(down_n):
+        combine(c, 0)
 
     halo.wait_send()
     to_relay(routes_ref, near_routes.at[my_turn], 0).wait_send()
@@ -614,7 +627,8 @@
 
         return 0
 
-    lax.fori_loop(0, down_n, end_down, 0)
+    for c in range(down_n):
+        end_down(c, 0)
 
     def end_go(i, _):
         go(partner(i), me).wait_send()
@@ -647,14 +661,14 @@
     rows_here, pool_width = pool_in.shape
     local = w_gate.shape[2]
     slots = ep_n * cap
-    down_n = 8
-    part = width // down_n
+    sizes = (width // 8,) * 8
+    down_n = len(sizes)
     gate_n = 8
     vmem = pl.BlockSpec(memory_space=pltpu.VMEM)
     hbm = pl.BlockSpec(memory_space=pl.ANY)
     dma = pltpu.SemaphoreType.DMA
     return pl.pallas_call(
-        functools.partial(kernel, (ep_n, tp_n, cap, gate_n, down_n)),
+        functools.partial(kernel, (ep_n, tp_n, cap, gate_n, sizes)),
         out_shape=(
             pltpu.VMEM((rows_here, width), BF16),
             pltpu.VMEM((block_rows, width), BF16),
@@ -676,12 +690,12 @@
             pltpu.VMEM((2, slots, local), F32),
             pltpu.VMEM((2, slots, local), F32),
             pltpu.VMEM((slots, tp_n * local), BF16),
-            pltpu.VMEM((down_n, tp_n * local, part), BF16),
-            pltpu.VMEM((down_n, ep_n, cap, part), BF16),
-            pltpu.VMEM((down_n, half, cap, part), BF16),
-            pltpu.VMEM((down_n, 2, half, cap, part), BF16),
-            pltpu.VMEM((down_n, 2, block_rows, part), BF16),
-            pltpu.VMEM((down_n, block_rows, part), BF16),
+            pltpu.VMEM((tp_n * local, width), BF16),
+            pltpu.VMEM((ep_n, cap, width), BF16),
+            pltpu.VMEM((half, cap, width), BF16),
+            pltpu.VMEM((2, half, cap, width), BF16),
+            pltpu.VMEM((2, block_rows, width), BF16),
+            pltpu.VMEM((block_rows, width), BF16),
             pltpu.VMEM((2, K, block_rows), jnp.int32),
             pltpu.VMEM((2, K, block_rows), F32),
             pltpu.VMEM((3, block_rows, half * cap), BF16),

time: 93.2 us -> 93 us (level)
  no operation moved by 1% of the time
where the time goes in v3:
time: 93 us; the launch traced here: 92.8 us
  Pallas kernels  90.4 us (97%)
  local copies, waits for them, and re-layouts  1.77 us (2%)
    pallas_call x1, Pallas kernels, on_device(): pl.pallas_call(functools.partial(kernel, (ep_n, tp_n, cap, gate_n, sizes)...  90.4 us

profile of v3, /device:TPU:0, one launch (start us, length us, event | category | flops | bytes accessed | tf_op | source)
XLA Modules:
  0.0 92.8 jit_solution(5401171084608193573)
XLA Ops:
  0.6 90.4 %shard_map.122 = (bf16[256,2048]{1,0:T(8,128)(2,1)S(1)}, bf16[128,2048]{1,0:T(8,128)(2,1)S(1)}) custom-call(s32[2,512]{1,0:T(2,128)} %bitcast.5, f32[2,512]{1,0:T(2,128)} %bitcast.6, f32[1,2048]{1,0:T(1,128)} %bitcast.4, f32[1,1024]{1,0:T(1,128)} %bitcast.7, bf16[8,128,128]{2,1,0:T(8,128)(2,1)} %wpool_hbm.1, bf16[256,1024]{1,0:T(8,128)(2,1)} %pool_hbm.1, ...), custom_call_target="tpu_custom_call" | custom-call | tf_op jit(solution)/shard_map/pallas_call | solution.py:670
  91.0 1.0 %copy.15 = bf16[256,2048]{1,0:T(8,128)(2,1)} copy(bf16[256,2048]{1,0:T(8,128)(2,1)S(1)} %get-tuple-element.2) | data formatting | bytes 2097152
  92.0 0.8 copy.16

commit v4 on v3

--- a/solution.py
+++ b/solution.py
@@ -506,7 +506,9 @@
         )
 
     def weighed(at, values):
-        return dot(merge_high[at], values) + dot(merge_low[at], values)
+        both = jnp.concatenate([merge_high[at], merge_low[at]], axis=0)
+        value = dot(both, values)
+        return value[:block_rows] + value[block_rows:]
 
     def pass_on(c):
         for k in range(2):
@@ -531,8 +533,11 @@
         far_down(c).wait_recv()
         relay_down(c).start()
         near_down(c).wait_recv()
+        held = 3 * local
+        value = dot(hidden[:, :held], down_all[:held, down_cols(c)])
         relay_down(c).wait_recv()
-        value = dot(hidden[...], down_all[:, down_cols(c)]).astype(BF16)
+        value = value + dot(hidden[:, held:], down_all[held:, down_cols(c)])
+        value = value.astype(BF16)
         result[:, :, down_cols(c)] = value.reshape(ep_n, cap, sizes[c])
 
         def start_group(i, _):

time: 93 us -> 93 us (level)
  no operation moved by 1% of the time
where the time goes in v4:
time: 93 us; the launch traced here: 92.8 us
  Pallas kernels  90.4 us (97%)
  local copies, waits for them, and re-layouts  1.77 us (2%)
    pallas_call x1, Pallas kernels, on_device(): pl.pallas_call(functools.partial(kernel, (ep_n, tp_n, cap, gate_n, sizes)...  90.4 us

profile of v4, /device:TPU:0, one launch (start us, length us, event | category | flops | bytes accessed | tf_op | source)
XLA Modules:
  0.0 92.8 jit_solution(536639730896767466)
XLA Ops:
  0.6 90.4 %shard_map.122 = (bf16[256,2048]{1,0:T(8,128)(2,1)S(1)}, bf16[128,2048]{1,0:T(8,128)(2,1)S(1)}) custom-call(s32[2,512]{1,0:T(2,128)} %bitcast.5, f32[2,512]{1,0:T(2,128)} %bitcast.6, f32[1,2048]{1,0:T(1,128)} %bitcast.4, f32[1,1024]{1,0:T(1,128)} %bitcast.7, bf16[8,128,128]{2,1,0:T(8,128)(2,1)} %wpool_hbm.1, bf16[256,1024]{1,0:T(8,128)(2,1)} %pool_hbm.1, ...), custom_call_target="tpu_custom_call" | custom-call | tf_op jit(solution)/shard_map/pallas_call | solution.py:675
  91.0 1.0 %copy.15 = bf16[256,2048]{1,0:T(8,128)(2,1)} copy(bf16[256,2048]{1,0:T(8,128)(2,1)S(1)} %get-tuple-element.2) | data formatting | bytes 2097152
  92.0 0.8 copy.16
